TPU v7x, 32 devices: a whole 2x2x4 slice. The times are simulated.
32 devices in a mesh: grp: 2 (over x), ep: 8 (over z, y), tp: 2 (over core).
Axes of the slice: x: 2, y: 2, z: 4, core: 2. Of those that a mesh axis runs over, the one named last changes fastest.
Arguments:
- tokens: bfloat16 [8192, 2048], P(('grp', 'ep', 'tp')), parts along dimension 0, may hold values from -6 to 6
- norm_gain: float32 [2048], replicated, may hold values from 0.1 to 1.9
- expert_ids: int32 [8192, 2], P(('grp', 'ep', 'tp')), parts along dimension 0, may hold values from 0 to 7, all different within a row; in each aligned block of 256 rows (0 to 255, 256 to 511, ...) at most 96 rows name the same one
- route_weights: float32 [8192, 2], P(('grp', 'ep', 'tp')), parts along dimension 0, may hold values from 0.05 to 1
- w_gate: bfloat16 [8, 2048, 1024], P('ep', None, 'tp'), may hold values from -0.125 to 0.125
- w_up: bfloat16 [8, 2048, 1024], P('ep', None, 'tp'), may hold values from -0.125 to 0.125
- w_down: bfloat16 [8, 1024, 2048], P('ep', 'tp'), may hold values from -0.1875 to 0.1875
Outputs:
- mixed: bfloat16 [8192, 2048], P(('grp', 'ep', 'tp')), parts along dimension 0
There are 2 independent parts, one for each index of `grp`. A program takes and returns all parts, laid end to end along the dimension named above; an argument that names none is the same for every part. Nothing has to cross between parts.
Inputs may be any that keep to these rules, and one draw needn't show every extreme that they name: `expert_ids`: each row names 2 different experts. Among the rows of one device no expert is named more than 96 times, and in every draw some expert is named exactly 96 times by the rows of some device.
All inputs are finite; a program needn't handle non-finite values.
Results may differ from a plain program's by a relative error of at most 0.0071.
Values may be sent and summed in bfloat16 or wider, within the bound.
A program may use at most 128 MiB of HBM per device.

v0:
```python
import jax
import jax.numpy as jnp
from jax import lax
from jax.sharding import PartitionSpec as P


def per_device(tokens, norm_gain, expert_ids, route_weights, w_gate, w_up, w_down):
    tok_rows = tokens.shape[0]
    top_count = expert_ids.shape[1]
    width = tokens.shape[1]
    local_experts = w_gate.shape[0]
    ep_size = lax.axis_size("ep")
    experts = local_experts * ep_size
    slots = 3 * tok_rows * top_count // (2 * experts)
    values = tokens.astype(jnp.float32)
    scale = lax.rsqrt(jnp.mean(values * values, axis=-1, keepdims=True) + 1e-06)
    normed = (values * scale * norm_gain).astype(jnp.bfloat16)
    flat_ids = expert_ids.reshape(-1)
    onehot = (flat_ids[:, None] == jnp.arange(experts, dtype=jnp.int32)[None, :]).astype(jnp.int32)
    before = jnp.cumsum(onehot, axis=0) - onehot
    slot_of = jnp.sum(before * onehot, axis=1)
    target = flat_ids * slots + slot_of
    owner = jnp.arange(tok_rows * top_count, dtype=jnp.int32) // top_count + 1
    source = jnp.zeros((experts * slots,), jnp.int32).at[target].set(owner)
    filled = source > 0
    picked = jnp.take(normed, jnp.maximum(source - 1, 0), axis=0)
    outgoing = jnp.where(filled[:, None], picked, jnp.zeros_like(picked))
    outgoing = outgoing.reshape(ep_size, local_experts, slots, width)
    gate_full, up_full = (
        lax.all_gather(w_gate, "tp", axis=2, tiled=True),
        lax.all_gather(w_up, "tp", axis=2, tiled=True),
    )
    down_full = lax.all_gather(w_down, "tp", axis=1, tiled=True)
    arrived = lax.all_to_all(outgoing, "ep", split_axis=0, concat_axis=0, tiled=True)
    senders, _, part_slots, _ = arrived.shape
    rows = jnp.transpose(arrived, (1, 0, 2, 3)).reshape(local_experts, senders * part_slots, width)
    gate = jnp.einsum("erd,edf->erf", rows, gate_full, preferred_element_type=jnp.float32)
    upper = jnp.einsum("erd,edf->erf", rows, up_full, preferred_element_type=jnp.float32)
    hidden = (jax.nn.silu(gate) * upper).astype(jnp.bfloat16)
    result = jnp.einsum(
        "erf,efd->erd", hidden, down_full, preferred_element_type=jnp.float32
    ).astype(jnp.bfloat16)
    result = result.reshape(local_experts, senders, part_slots, width)
    result = jnp.transpose(result, (1, 0, 2, 3))
    results = lax.all_to_all(result, "ep", split_axis=0, concat_axis=0, tiled=True)
    results = results.reshape(experts * slots, width)
    gathered = jnp.take(results, target, axis=0).reshape(tok_rows, top_count, width)
    mixed = jnp.sum(route_weights[:, :, None] * gathered.astype(jnp.float32), axis=1)
    return mixed.astype(jnp.bfloat16)


def solution(mesh):
    in_specs = (
        P(("grp", "ep", "tp"), None),
        P(),
        P(("grp", "ep", "tp"), None),
        P(("grp", "ep", "tp"), None),
        P("ep", None, "tp"),
        P("ep", None, "tp"),
        P("ep", "tp", None),
    )
    out_specs = P(("grp", "ep", "tp"), None)
    return jax.shard_map(
        per_device, mesh=mesh, in_specs=in_specs, out_specs=out_specs, check_vma=False
    )
```

profile of v0, /device:TPU:0, one launch (start us, length us, event | category | flops | bytes accessed | tf_op | source)
XLA Modules:
  0.0 219.2 jit_solution(475283802855415070)
XLA Ops:
  6.5 0.0 copy-start.1
  6.5 0.0 copy-start
  6.5 0.0 copy-start.2
  6.5 0.0 all-gather.6.cloned.1.call-start
  6.5 0.7 all-gather.6.cloned.1.call-update
  7.3 0.0 all-gather.4.cloned.1.call-start
  7.3 0.7 all-gather.4.cloned.1.call-update
  8.0 0.0 copy-done.1
  8.0 0.1 copy.21
  8.2 0.1 eq.26
  8.3 0.1 reshape.138
  8.5 1.1 reduce-window.6
  9.6 0.2 slice_reduce_fusion
  9.9 0.1 copy.25
  10.0 0.1 mul.62
  10.2 0.1 fusion.15
  10.3 2.4 %scatter_custom_fusion = s32[768]{0:T(1024)S(1)} fusion(s32[512]{0:T(512)S(1)} %bitcast.40, s32[512]{0:T(512)S(1)} %fusion.17, s32[]{:T(128)} %constant.59.clone.1), kind=kCustom, calls=%fused_computation.41 | custom fusion | bytes 3076 | tf_op jit(solution)/shard_map/scatter | solution.py:24
  12.8 0.1 broadcast_in_dim.44
  12.8 0.1 broadcast_in_dim.46
  12.9 0.0 copy-done
  12.9 0.3 fusion.11
  13.2 0.0 copy-done.2
  13.2 0.3 fusion.13
  13.6 4.3 %gather_fusion = bf16[768,2048]{1,0:T(8,128)(2,1)} fusion(bf16[256,2048]{1,0:T(8,128)(2,1)S(1)} %fusion.13, s32[1024]{0:T(1024)S(1)} %pad_clamp_fusion.1), kind=kCustom, calls=%fused_computation | custom fusion | bytes 6294528 | tf_op jit(solution)/shard_map/jit(_take)/gather | solution.py:26
  17.9 3.7 %select_select_fusion = bf16[8,1,96,2048]{3,2,1,0:T(8,128)(2,1)} fusion(bf16[8,1,96,2048]{3,2,1,0:T(8,128)(2,1)} %bitcast.35, pred[8,96]{1,0:T(8,128)(4,1)S(1)} %broadcast_in_dim.46, pred[8,96]{1,0:T(8,128)(4,1)S(1)} %broadcast_in_dim.44), kind=kLoop, calls=%fused_computation.13 | loop fusion | flops 3145728 | bytes 6292992 | tf_op jit(solution)/shard_map/jit(_where)/select_n | solution.py:27
  21.6 7.4 %all-to-all-start = ((bf16[8,1,96,2048]{3,2,1,0:T(8,128)(2,1)}), bf16[8,1,96,2048]{3,2,1,0:T(8,128)(2,1)S(1)}, u32[]{:S(2)}, u32[]{:S(2)}) async-start(bf16[8,1,96,2048]{3,2,1,0:T(8,128)(2,1)} %select_select_fusion), calls=%async_computation | async-start | bytes 6291456 | tf_op jit(solution)/shard_map/all_to_all | solution.py:34
  29.0 0.0 all-gather.8.cloned.1.call-start
  29.1 0.7 all-gather.8.cloned.1.call-update
  29.8 0.0 all-gather.6.cloned.1.call-done
  29.8 69.9 %all-to-all-done = bf16[8,1,96,2048]{3,2,1,0:T(8,128)(2,1)S(1)} async-done(((bf16[8,1,96,2048]{3,2,1,0:T(8,128)(2,1)}), bf16[8,1,96,2048]{3,2,1,0:T(8,128)(2,1)S(1)}, u32[]{:S(2)}, u32[]{:S(2)}) %all-to-all-start) | async-done | bytes 3145760 | tf_op jit(solution)/shard_map/all_to_all | solution.py:34
  99.7 7.3 %fusion.2 = f32[768,1024]{1,0:T(8,128)} fusion(bf16[768,2048]{1,0:T(8,128)(2,1)S(1)} %bitcast.36, bf16[1,2048,1024]{2,1,0:T(8,128)(2,1)} %all-gather.6.cloned.1.call-done), kind=kOutput, calls=%fused_computation.5 | convolution fusion | flops 3221225472 | bytes 10485760 | tf_op jit(solution)/shard_map/erd,edf->erf/dot_general | solution.py:38
  107.0 0.0 all-gather.4.cloned.1.call-done
  107.0 7.5 %multiply_convert_fusion = bf16[768,1024]{1,0:T(8,128)(2,1)} fusion(f32[768,1024]{1,0:T(8,128)} %fusion.2, bf16[768,2048]{1,0:T(8,128)(2,1)S(1)} %bitcast.37, bf16[1,2048,1024]{2,1,0:T(8,128)(2,1)} %all-gather.4.cloned.1.call-done), kind=kOutput, calls=%fused_computation.12 | convolution fusion | flops 3225944064 | bytes 12058624 | tf_op jit(solution)/shard_map/erd,edf->erf/dot_general | solution.py:37
  114.5 0.0 all-gather.8.cloned.1.call-done
  114.5 7.7 %fusion.6 = bf16[768,2048]{1,0:T(8,128)(2,1)} fusion(bf16[768,1024]{1,0:T(8,128)(2,1)} %multiply_convert_fusion, bf16[1,1024,2048]{2,1,0:T(8,128)(2,1)} %all-gather.8.cloned.1.call-done), kind=kOutput, calls=%fused_computation.11 | convolution fusion | flops 3222798336 | bytes 8912896 | tf_op jit(solution)/shard_map/erf,efd->erd/dot_general | solution.py:40
  122.3 0.0 copy-start.3
  122.3 4.0 %all-to-all-start.1 = ((bf16[8,1,96,2048]{3,2,1,0:T(8,128)(2,1)}), bf16[8,1,96,2048]{3,2,1,0:T(8,128)(2,1)S(1)}, u32[]{:S(2)}, u32[]{:S(2)}) async-start(bf16[8,1,96,2048]{3,2,1,0:T(8,128)(2,1)} %bitcast.38), calls=%async_computation.1 | async-start | bytes 6291456 | tf_op jit(solution)/shard_map/all_to_all | solution.py:45
  126.2 0.1 reduce_sum.32
  126.4 0.1 copy.23
  126.5 0.2 copy.24
  126.7 0.0 copy-done.3
  126.7 0.1 copy.20
  126.8 70.2 %all-to-all-done.1 = bf16[8,1,96,2048]{3,2,1,0:T(8,128)(2,1)S(1)} async-done(((bf16[8,1,96,2048]{3,2,1,0:T(8,128)(2,1)}), bf16[8,1,96,2048]{3,2,1,0:T(8,128)(2,1)S(1)}, u32[]{:S(2)}, u32[]{:S(2)}) %all-to-all-start.1) | async-done | bytes 3145760 | tf_op jit(solution)/shard_map/all_to_all | solution.py:45
  197.0 3.3 %gather_fusion.1 = bf16[512,2048]{1,0:T(8,128)(2,1)} fusion(bf16[768,2048]{1,0:T(8,128)(2,1)S(1)} %bitcast.34, s32[1024]{0:T(1024)S(1)} %pad_clamp_fusion), kind=kCustom, calls=%fused_computation.1 | custom fusion | bytes 4196352 | tf_op jit(solution)/shard_map/jit(_take)/gather | solution.py:47
  200.3 3.2 %gather.15 = bf16[256,2,2048]{2,1,0:T(2,128)(2,1)S(1)} reshape(bf16[512,2048]{1,0:T(8,128)(2,1)} %gather_fusion.1) | data formatting | bytes 4194304 | tf_op jit(solution)/shard_map/jit(_take)/gather | solution.py:47
  203.5 9.2 %multiply_reduce_fusion = bf16[256,2048]{1,0:T(8,128)(2,1)} fusion(bf16[256,2,2048]{2,1,0:T(2,128)(2,1)S(1)} %gather.15, pred[256,2]{1,0:T(8,128)(4,1)S(1)} %copy.24, f32[256,2]{1,0:T(8,128)S(1)} %copy.20), kind=kLoop, calls=%fused_computation.9 | loop fusion | flops 3670016 | bytes 3148288 | tf_op jit(solution)/shard_map/reduce_sum | solution.py:48
  (12 shorter events, 0.1 us)
Async XLA Ops:
  6.5 1.5 copy-start.1
  6.5 6.4 %copy-start = (bf16[256,2048]{1,0:T(8,128)(2,1)S(1)}, bf16[256,2048]{1,0:T(8,128)(2,1)}, u32[]{:S(2)}) copy-start(bf16[256,2048]{1,0:T(8,128)(2,1)} %param.7) | copy-start | bytes 3145732
  6.5 6.7 %copy-start.2 = (f32[2048]{0:T(1024)S(1)}, f32[2048]{0:T(1024)}, u32[]{:S(2)}) copy-start(f32[2048]{0:T(1024)} %param.8) | copy-start | bytes 24580
  6.5 23.3 %all-gather.6.cloned.1.call-start = ((), (), s32[]{:S(2)}) async-start(), calls=%async_computation.3 | async-start | bytes 6291456 | tf_op jit(solution)/shard_map/all_gather | solution.py:31
  7.3 99.7 %all-gather.4.cloned.1.call-start = ((), (), s32[]{:S(2)}) async-start(), calls=%async_computation.2 | async-start | bytes 6291456 | tf_op jit(solution)/shard_map/all_gather | solution.py:30
  21.6 78.1 %all-to-all-start = ((bf16[8,1,96,2048]{3,2,1,0:T(8,128)(2,1)}), bf16[8,1,96,2048]{3,2,1,0:T(8,128)(2,1)S(1)}, u32[]{:S(2)}, u32[]{:S(2)}) async-start(bf16[8,1,96,2048]{3,2,1,0:T(8,128)(2,1)} %select_select_fusion), calls=%async_computation | async-start | bytes 6291456 | tf_op jit(solution)/shard_map/all_to_all | solution.py:34
  29.0 85.5 %all-gather.8.cloned.1.call-start = ((), (), s32[]{:S(2)}) async-start(), calls=%async_computation.4 | async-start | bytes 6291456 | tf_op jit(solution)/shard_map/all_gather | solution.py:33
  122.3 4.4 %copy-start.3 = (f32[256,2]{0,1:T(2,128)S(1)}, f32[256,2]{0,1:T(2,128)}, u32[]{:S(2)}) copy-start(f32[256,2]{0,1:T(2,128)} %param.10) | copy-start | bytes 6148
  122.3 74.7 %all-to-all-start.1 = ((bf16[8,1,96,2048]{3,2,1,0:T(8,128)(2,1)}), bf16[8,1,96,2048]{3,2,1,0:T(8,128)(2,1)S(1)}, u32[]{:S(2)}, u32[]{:S(2)}) async-start(bf16[8,1,96,2048]{3,2,1,0:T(8,128)(2,1)} %bitcast.38), calls=%async_computation.1 | async-start | bytes 6291456 | tf_op jit(solution)/shard_map/all_to_all | solution.py:45
Sparse Core Ops, SparseCore 0:
  8.9 16.3 all-gather.5
  26.8 14.8 all-gather.3
  43.3 14.8 all-gather.7
where the time goes:
time: 220 us; the launch traced here: 219 us
  waiting for transfers between devices  142 us (65%)
  matrix products  22.5 us (10%)
  local copies, waits for them, and re-layouts  14.9 us (7%)
  other arithmetic  14.9 us (7%)
  between operations  13.3 us (6%)
  starting transfers between devices  11.4 us (5%)
    all_to_all x1, waiting for transfers between devices, per_device(): lax.all_to_all(result, 'ep', split_axis=0, concat_axis=0, tiled=True)  70.2 us
    all_to_all x1, waiting for transfers between devices, per_device(): lax.all_to_all(outgoing, 'ep', split_axis=0, concat_axis=0, tiled=True)  69.9 us
    reduce_sum x1, other arithmetic, per_device(): jnp.sum(route_weights[:, :, None] * gathered.astype(jnp.float32), axis=1)  9.21 us
    dot_general x1, matrix products, per_device(): jnp.einsum('erf,efd->erd', hidden, down_full, preferred_element_type=jnp....  7.75 us
    dot_general x1, matrix products, per_device(): jnp.einsum('erd,edf->erf', rows, gate_full, preferred_element_type=jnp.fl...  7.51 us
    all_to_all x1, starting transfers between devices, per_device(): lax.all_to_all(outgoing, 'ep', split_axis=0, concat_axis=0, tiled=True)  7.4 us
    dot_general x1, matrix products, per_device(): jnp.einsum('erd,edf->erf', rows, up_full, preferred_element_type=jnp.floa...  7.27 us
    gather x2, local copies, waits for them, and re-layouts, per_device(): jnp.take(results, target, axis=0).reshape(tok_rows, top_count, width)  6.5 us
  transfers between devices with their start and end apart: 5, of which 2 were waited for; matrix products, arithmetic and copies ran while one was open for 13% of the time, Pallas kernels for 0%

commit v1 on v0

--- a/solution.py
+++ b/solution.py
@@ -1,10 +1,18 @@
+import functools
+
 import jax
 import jax.numpy as jnp
 from jax import lax
+from jax.experimental import pallas as pl
+from jax.experimental.pallas import tpu as pltpu
 from jax.sharding import PartitionSpec as P
 
-
-def per_device(tokens, norm_gain, expert_ids, route_weights, w_gate, w_up, w_down):
+MESH = pl.DeviceIdType.MESH
+F32 = jnp.float32
+BF16 = jnp.bfloat16
+
+
+def plain_device(tokens, norm_gain, expert_ids, route_weights, w_gate, w_up, w_down):
     tok_rows = tokens.shape[0]
     top_count = expert_ids.shape[1]
     width = tokens.shape[1]
@@ -49,6 +57,220 @@
     return mixed.astype(jnp.bfloat16)
 
 
+def flip(me, d, ep):
+    out, bit = 0, 1
+    while bit < ep:
+        out = out + bit * ((me // bit + d // bit) % 2)
+        bit *= 2
+    return out
+
+
+def kernel(
+    ep, slots, tok, gain, ids, rw, wg, wu, wd, o_ref,
+    gbuf, ubuf, dbuf, normed, out, recv, hid, res, back, acc,
+    w_sem, ws_sem, wr_sem, s1, r1, s2, r2,
+):
+    me = lax.axis_index("ep")
+    tp = lax.axis_index("tp")
+    rows, width = tok.shape
+    half = wg.shape[2]
+    tile = min(512, width)
+    mine = pl.ds(pl.multiple_of(tp * half, 128), half)
+
+    barrier = pltpu.get_barrier_semaphore()
+    for d in range(1, ep):
+        pl.semaphore_signal(barrier, inc=1, device_id={"ep": flip(me, d, ep)}, device_id_type=MESH)
+    pl.semaphore_signal(barrier, inc=1, device_id={"tp": 1 - tp}, device_id_type=MESH)
+
+    weights = [
+        (wg.at[0], gbuf.at[tp]),
+        (wu.at[0], ubuf.at[tp]),
+        (wd.at[0], dbuf.at[mine]),
+    ]
+    local = [pltpu.make_async_copy(a, b, w_sem.at[i]) for i, (a, b) in enumerate(weights)]
+    for c in local:
+        c.start()
+
+    @pl.loop(0, rows // 16)
+    def _(i):
+        at = pl.ds(pl.multiple_of(i * 16, 16), 16)
+        v = tok[at, :].astype(F32)
+        scale = lax.rsqrt(jnp.mean(v * v, axis=-1, keepdims=True) + 1e-06)
+        normed[at, :] = (v * scale * gain[...]).astype(BF16)
+
+    lane = lax.broadcasted_iota(jnp.int32, (rows, 128), 1)
+    rel = ids[...] ^ me
+    hits = [rel[:, k:k + 1] == lane for k in range(ids.shape[1])]
+    member = jnp.zeros((rows, 128), F32)
+    share = jnp.zeros((rows, 128), F32)
+    for k, hit in enumerate(hits):
+        member = member + jnp.where(hit, 1.0, 0.0)
+        share = share + jnp.where(hit, rw[:, k:k + 1], 0.0)
+    later = lax.broadcasted_iota(jnp.int32, (rows, rows), 0)
+    earlier = lax.broadcasted_iota(jnp.int32, (rows, rows), 1)
+    below = jnp.where(earlier < later, 1.0, 0.0).astype(BF16)
+    rank = jnp.dot(below, member.astype(BF16), preferred_element_type=F32)
+    key = member * (rank + 1.0) - 1.0
+    key_t = key.T
+    key = key.astype(jnp.int32)
+    key_t = key_t.astype(jnp.int32)
+
+    def pick(d, dst, base):
+        spot = lax.broadcasted_iota(jnp.int32, (slots, rows), 0)
+        sel = jnp.where(spot == key_t[d:d + 1, :], 1.0, 0.0).astype(BF16)
+
+        @pl.loop(0, width // tile)
+        def _(j):
+            c = pl.ds(pl.multiple_of(j * tile, tile), tile)
+            dst[pl.ds(base, slots), c] = jnp.dot(
+                sel, normed[:, c], preferred_element_type=F32
+            ).astype(BF16)
+
+    def send_rows(d):
+        at = pl.ds(pl.multiple_of(d * slots, 16), slots)
+        return pltpu.make_async_remote_copy(
+            src_ref=out.at[at], dst_ref=recv.at[at], send_sem=s1.at[d], recv_sem=r1.at[d],
+            device_id={"ep": flip(me, d, ep)}, device_id_type=MESH,
+        )
+
+    def send_back(d):
+        at = pl.ds(pl.multiple_of(d * slots, 16), slots)
+        return pltpu.make_async_remote_copy(
+            src_ref=res.at[at], dst_ref=back.at[at], send_sem=s2.at[d], recv_sem=r2.at[d],
+            device_id={"ep": flip(me, d, ep)}, device_id_type=MESH,
+        )
+
+    pl.semaphore_wait(barrier, ep)
+
+    order = range(1, ep)
+    for d in order:
+        pick(d, out, d * slots)
+        send_rows(d).start()
+    passed = [
+        pltpu.make_async_remote_copy(
+            src_ref=a, dst_ref=b, send_sem=ws_sem.at[i], recv_sem=wr_sem.at[i],
+            device_id={"tp": 1 - tp}, device_id_type=MESH,
+        )
+        for i, (a, b) in enumerate(weights)
+    ]
+    for c in passed:
+        c.start()
+    pick(0, recv, 0)
+    for c in local:
+        c.wait()
+    for c in passed:
+        c.wait_recv()
+
+    def work(p):
+        at = pl.ds(pl.multiple_of(p * 2 * slots, 16), 2 * slots)
+        nt = 256
+        for h in range(2):
+            for n in range(half // nt):
+                c = slice(n * nt, (n + 1) * nt)
+                x = recv[at, :]
+                g = jnp.dot(x, gbuf[h, :, c], preferred_element_type=F32)
+                u = jnp.dot(x, ubuf[h, :, c], preferred_element_type=F32)
+                v = g / (1.0 + jnp.exp(-g)) * u
+                hid[:, h * half + n * nt:h * half + (n + 1) * nt] = v.astype(BF16)
+
+        @pl.loop(0, width // tile)
+        def _(j):
+            c = pl.ds(pl.multiple_of(j * tile, tile), tile)
+            res[at, c] = jnp.dot(hid[...], dbuf[:, c], preferred_element_type=F32).astype(BF16)
+
+    send_rows(1).wait_recv()
+    work(0)
+    send_back(1).start()
+
+    @pl.loop(1, ep // 2)
+    def _(p):
+        send_rows(2 * p).wait_recv()
+        send_rows(2 * p + 1).wait_recv()
+        work(p)
+        send_back(2 * p).start()
+        send_back(2 * p + 1).start()
+
+    def mix(d, src):
+        slot = lax.broadcasted_iota(jnp.int32, (rows, slots), 1)
+        sel = jnp.where(slot == key[:, d:d + 1], 1.0, 0.0).astype(BF16)
+        part = share[:, d:d + 1]
+
+        @pl.loop(0, width // tile)
+        def _(j):
+            c = pl.ds(pl.multiple_of(j * tile, tile), tile)
+            y = part * jnp.dot(
+                sel, src[pl.ds(d * slots, slots), c], preferred_element_type=F32
+            )
+            if d == 0:
+                acc[:, c] = y
+            elif d < ep - 1:
+                acc[:, c] = acc[:, c] + y
+            else:
+                o_ref[:, c] = (acc[:, c] + y).astype(BF16)
+
+    mix(0, res)
+    for d in range(1, ep):
+        send_back(d).wait_recv()
+        mix(d, back)
+    for d in range(1, ep):
+        send_rows(d).wait_send()
+        send_back(d).wait_send()
+    for c in passed:
+        c.wait_send()
+
+
+def fused_device(tokens, norm_gain, expert_ids, route_weights, w_gate, w_up, w_down):
+    rows, width = tokens.shape
+    ep = lax.axis_size("ep")
+    tps = lax.axis_size("tp")
+    slots = 3 * rows * expert_ids.shape[1] // (2 * ep)
+    half = w_gate.shape[2]
+    vm = pl.BlockSpec(memory_space=pltpu.VMEM)
+    anywhere = pl.BlockSpec(memory_space=pl.ANY)
+    dma = pltpu.SemaphoreType.DMA
+    return pl.pallas_call(
+        functools.partial(kernel, ep, slots),
+        out_shape=jax.ShapeDtypeStruct((rows, width), BF16),
+        in_specs=[vm, vm, vm, vm, anywhere, anywhere, anywhere],
+        out_specs=vm,
+        scratch_shapes=[
+            pltpu.VMEM((tps, width, half), BF16),
+            pltpu.VMEM((tps, width, half), BF16),
+            pltpu.VMEM((tps * half, width), BF16),
+            pltpu.VMEM((rows, width), BF16),
+            pltpu.VMEM((ep * slots, width), BF16),
+            pltpu.VMEM((ep * slots, width), BF16),
+            pltpu.VMEM((2 * slots, tps * half), BF16),
+            pltpu.VMEM((ep * slots, width), BF16),
+            pltpu.VMEM((ep * slots, width), BF16),
+            pltpu.VMEM((rows, width), F32),
+            dma((3,)), dma((3,)), dma((3,)),
+            dma((ep,)), dma((ep,)), dma((ep,)), dma((ep,)),
+        ],
+        compiler_params=pltpu.CompilerParams(
+            collective_id=0, has_side_effects=True, vmem_limit_bytes=56 * 1024 * 1024
+        ),
+    )(tokens, norm_gain.reshape(1, -1), expert_ids, route_weights, w_gate, w_up, w_down)
+
+
+def per_device(tokens, norm_gain, expert_ids, route_weights, w_gate, w_up, w_down):
+    rows, width = tokens.shape
+    ep = lax.axis_size("ep")
+    slots = 3 * rows * expert_ids.shape[1] // (2 * ep)
+    fits = (
+        w_gate.shape[0] == 1
+        and lax.axis_size("tp") == 2
+        and ep & (ep - 1) == 0
+        and ep <= 128
+        and slots % 16 == 0
+        and rows % 128 == 0
+        and width % 512 == 0
+        and w_gate.shape[2] % 256 == 0
+    )
+    body = fused_device if fits else plain_device
+    return body(tokens, norm_gain, expert_ids, route_weights, w_gate, w_up, w_down)
+
+
 def solution(mesh):
     in_specs = (
         P(("grp", "ep", "tp"), None),

time: 220 us -> 158 us (0.72)
  the two profiles are of different devices: /device:TPU:0 before, /device:TPU:10 now
where the time goes in v1:
time: 158 us
  Pallas kernels  152 us (96%)
  local copies, waits for them, and re-layouts  5.24 us (3%)
    pallas_call x1, Pallas kernels, fused_device(): pl.pallas_call(functools.partial(kernel, ep, slots), out_shape=jax.ShapeD...  152 us
    unnamed x3, local copies, waits for them, and re-layouts  5.24 us

profile of v1, /device:TPU:10, one launch (start us, length us, event | category | flops | bytes accessed | tf_op | source)
XLA Modules:
  0.0 157.8 jit_solution(13317182696207189429)
XLA Ops:
  0.0 1.5 copy.8.ids
  1.5 1.5 copy.9.rw
  2.9 152.5 %shard_map.73 = bf16[256,2048]{1,0:T(8,128)(2,1)} custom-call(bf16[256,2048]{1,0:T(8,128)(2,1)} %tok.1, f32[1,2048]{1,0:T(1,128)} %bitcast.1, s32[256,2]{1,0:T(8,128)} %copy.8.ids, f32[256,2]{1,0:T(8,128)} %copy.9.rw, bf16[1,2048,512]{2,1,0:T(8,128)(2,1)} %wg.1, bf16[1,2048,512]{2,1,0:T(8,128)(2,1)} %wu.1, bf16[1,512,2048]{2,1,0:T(8,128)(2,1)} %wd.1), custom_call_target="tpu_custom_call" | custom-call | tf_op jit(solution)/shard_map/pallas_call | solution.py:231
  155.4 2.3 %copy.11 = bf16[256,2048]{1,0:T(8,128)(2,1)} copy(bf16[256,2048]{1,0:T(8,128)(2,1)} %shard_map.73) | data formatting | bytes 2097152

commit v2 on v1

--- a/solution.py
+++ b/solution.py
@@ -68,10 +68,13 @@
 def kernel(
     ep, slots, tok, gain, ids, rw, wg, wu, wd, o_ref,
     gbuf, ubuf, dbuf, normed, out, recv, hid, res, back, acc,
-    w_sem, ws_sem, wr_sem, s1, r1, s2, r2,
+    meta, meta_in, joined, joined_in,
+    w_sem, ws_sem, wr_sem, s1, r1, s2, r2, s3, r3,
 ):
     me = lax.axis_index("ep")
     tp = lax.axis_index("tp")
+    far = ep // 2
+    inner = (me // (far // 2) + me // far) % 2
     rows, width = tok.shape
     half = wg.shape[2]
     tile = min(512, width)
@@ -112,6 +115,8 @@
     rank = jnp.dot(below, member.astype(BF16), preferred_element_type=F32)
     key = member * (rank + 1.0) - 1.0
     key_t = key.T
+    meta[0:ep, :] = key_t[0:ep, :]
+    meta[ep:2 * ep, :] = share.T[0:ep, :]
     key = key.astype(jnp.int32)
     key_t = key_t.astype(jnp.int32)
 
@@ -133,17 +138,32 @@
             device_id={"ep": flip(me, d, ep)}, device_id_type=MESH,
         )
 
-    def send_back(d):
+    def send_back(d, to):
         at = pl.ds(pl.multiple_of(d * slots, 16), slots)
         return pltpu.make_async_remote_copy(
             src_ref=res.at[at], dst_ref=back.at[at], send_sem=s2.at[d], recv_sem=r2.at[d],
-            device_id={"ep": flip(me, d, ep)}, device_id_type=MESH,
+            device_id={"ep": flip(me, to, ep)}, device_id_type=MESH,
+        )
+
+    def across(i, src, dst):
+        return pltpu.make_async_remote_copy(
+            src_ref=src, dst_ref=dst, send_sem=s3.at[i], recv_sem=r3.at[i],
+            device_id={"ep": flip(me, far, ep)}, device_id_type=MESH,
         )
 
     pl.semaphore_wait(barrier, ep)
 
-    order = range(1, ep)
-    for d in order:
+    told = across(0, meta, meta_in)
+    told.start()
+    distant = [d for p in reversed(range(far, ep, 2)) for d in (p, p + 1)]
+    for d in distant:
+        pick(d, out, d * slots)
+
+        @pl.when(inner == 1)
+        def _():
+            send_rows(d).start()
+
+    for d in range(1, far):
         pick(d, out, d * slots)
         send_rows(d).start()
     passed = [
@@ -180,41 +200,87 @@
 
     send_rows(1).wait_recv()
     work(0)
-    send_back(1).start()
-
-    @pl.loop(1, ep // 2)
+    send_back(1, 1).start()
+
+    @pl.loop(1, far // 2)
     def _(p):
         send_rows(2 * p).wait_recv()
         send_rows(2 * p + 1).wait_recv()
         work(p)
-        send_back(2 * p).start()
-        send_back(2 * p + 1).start()
-
-    def mix(d, src):
+        send_back(2 * p, 2 * p).start()
+        send_back(2 * p + 1, 2 * p + 1).start()
+
+    @pl.when(inner == 0)
+    def _():
+        for d in distant:
+            send_rows(d).start()
+
+    pairs = ep // 4
+
+    @pl.loop(0, pairs)
+    def _(i):
+        q = (i + inner) % pairs
+        d = far + 2 * q
+        send_rows(d).wait_recv()
+        send_rows(d + 1).wait_recv()
+        work(far // 2 + q)
+
+        @pl.when(q > 0)
+        def _():
+            send_back(d, 2 * q).start()
+
+        send_back(d + 1, 2 * q + 1).start()
+
+    def mix(d, src, slot_of, part_of, first, dst):
         slot = lax.broadcasted_iota(jnp.int32, (rows, slots), 1)
-        sel = jnp.where(slot == key[:, d:d + 1], 1.0, 0.0).astype(BF16)
-        part = share[:, d:d + 1]
+        sel = jnp.where(slot == slot_of[:, d:d + 1], 1.0, 0.0).astype(BF16)
 
         @pl.loop(0, width // tile)
         def _(j):
             c = pl.ds(pl.multiple_of(j * tile, tile), tile)
-            y = part * jnp.dot(
+            y = part_of * jnp.dot(
                 sel, src[pl.ds(d * slots, slots), c], preferred_element_type=F32
             )
-            if d == 0:
+            if not first:
+                y = acc[:, c] + y
+            if dst is None:
                 acc[:, c] = y
-            elif d < ep - 1:
-                acc[:, c] = acc[:, c] + y
             else:
-                o_ref[:, c] = (acc[:, c] + y).astype(BF16)
-
-    mix(0, res)
-    for d in range(1, ep):
-        send_back(d).wait_recv()
-        mix(d, back)
+                dst[:, c] = y.astype(BF16)
+
+    told.wait_recv()
+    blank = jnp.zeros((128 - 2 * ep, rows), F32)
+    theirs = jnp.concatenate([meta_in[...], blank], axis=0).T
+    slot_theirs = theirs.astype(jnp.int32)
+    for d in range(far, ep):
+        if d > far:
+            send_back(d, d - far).wait_recv()
+        mix(
+            d, res if d == far else back, slot_theirs, theirs[:, ep + d:ep + d + 1],
+            d == far, joined if d == ep - 1 else None,
+        )
+    home = across(1, joined, joined_in)
+    home.start()
+
+    for d in range(far):
+        if d > 0:
+            send_back(d, d).wait_recv()
+        mix(d, res if d == 0 else back, key, share[:, d:d + 1], d == 0, None)
+    home.wait_recv()
+
+    @pl.loop(0, width // tile)
+    def _(j):
+        c = pl.ds(pl.multiple_of(j * tile, tile), tile)
+        o_ref[:, c] = (acc[:, c] + joined_in[:, c].astype(F32)).astype(BF16)
+
     for d in range(1, ep):
         send_rows(d).wait_send()
-        send_back(d).wait_send()
+        if d < far:
+            send_back(d, d).wait_send()
+        elif d > far:
+            send_back(d, d - far).wait_send()
+    told.wait_send()
+    home.wait_send()
     for c in passed:
         c.wait_send()
 
@@ -244,8 +310,12 @@
             pltpu.VMEM((ep * slots, width), BF16),
             pltpu.VMEM((ep * slots, width), BF16),
             pltpu.VMEM((rows, width), F32),
+            pltpu.VMEM((2 * ep, rows), F32),
+            pltpu.VMEM((2 * ep, rows), F32),
+            pltpu.VMEM((rows, width), BF16),
+            pltpu.VMEM((rows, width), BF16),
             dma((3,)), dma((3,)), dma((3,)),
-            dma((ep,)), dma((ep,)), dma((ep,)), dma((ep,)),
+            dma((ep,)), dma((ep,)), dma((ep,)), dma((ep,)), dma((2,)), dma((2,)),
         ],
         compiler_params=pltpu.CompilerParams(
             collective_id=0, has_side_effects=True, vmem_limit_bytes=56 * 1024 * 1024
@@ -261,7 +331,7 @@
         w_gate.shape[0] == 1
         and lax.axis_size("tp") == 2
         and ep & (ep - 1) == 0
-        and ep <= 128
+        and 8 <= ep <= 32
         and slots % 16 == 0
         and rows % 128 == 0
         and width % 512 == 0

time: 158 us -> 156 us (0.987)
  the two profiles are of different devices: /device:TPU:10 before, /device:TPU:0 now
where the time goes in v2:
time: 156 us; the launch traced here: 155 us
  Pallas kernels  150 us (96%)
  local copies, waits for them, and re-layouts  5.24 us (3%)
    pallas_call x1, Pallas kernels, fused_device(): pl.pallas_call(functools.partial(kernel, ep, slots), out_shape=jax.ShapeD...  150 us
    unnamed x3, local copies, waits for them, and re-layouts  5.24 us

profile of v2, /device:TPU:0, one launch (start us, length us, event | category | flops | bytes accessed | tf_op | source)
XLA Modules:
  0.0 155.3 jit_solution(11398489820150246590)
XLA Ops:
  0.0 1.5 copy.8.ids
  1.5 1.5 copy.9.rw
  2.9 150.1 %shard_map.73 = bf16[256,2048]{1,0:T(8,128)(2,1)} custom-call(bf16[256,2048]{1,0:T(8,128)(2,1)} %tok.1, f32[1,2048]{1,0:T(1,128)} %bitcast.1, s32[256,2]{1,0:T(8,128)} %copy.8.ids, f32[256,2]{1,0:T(8,128)} %copy.9.rw, bf16[1,2048,512]{2,1,0:T(8,128)(2,1)} %wg.1, bf16[1,2048,512]{2,1,0:T(8,128)(2,1)} %wu.1, bf16[1,512,2048]{2,1,0:T(8,128)(2,1)} %wd.1), custom_call_target="tpu_custom_call" | custom-call | tf_op jit(solution)/shard_map/pallas_call | solution.py:297
  153.0 2.3 %copy.11 = bf16[256,2048]{1,0:T(8,128)(2,1)} copy(bf16[256,2048]{1,0:T(8,128)(2,1)} %shard_map.73) | data formatting | bytes 2097152

commit v3 on v2

--- a/solution.py
+++ b/solution.py
@@ -155,6 +155,9 @@
 
     told = across(0, meta, meta_in)
     told.start()
+    for d in range(1, far):
+        pick(d, out, d * slots)
+        send_rows(d).start()
     distant = [d for p in reversed(range(far, ep, 2)) for d in (p, p + 1)]
     for d in distant:
         pick(d, out, d * slots)
@@ -162,10 +165,6 @@
         @pl.when(inner == 1)
         def _():
             send_rows(d).start()
-
-    for d in range(1, far):
-        pick(d, out, d * slots)
-        send_rows(d).start()
     passed = [
         pltpu.make_async_remote_copy(
             src_ref=a, dst_ref=b, send_sem=ws_sem.at[i], recv_sem=wr_sem.at[i],
@@ -202,6 +201,11 @@
     work(0)
     send_back(1, 1).start()
 
+    @pl.when(inner == 0)
+    def _():
+        for d in distant:
+            send_rows(d).start()
+
     @pl.loop(1, far // 2)
     def _(p):
         send_rows(2 * p).wait_recv()
@@ -209,11 +213,6 @@
         work(p)
         send_back(2 * p, 2 * p).start()
         send_back(2 * p + 1, 2 * p + 1).start()
-
-    @pl.when(inner == 0)
-    def _():
-        for d in distant:
-            send_rows(d).start()
 
     pairs = ep // 4
 

time: 156 us -> 162 us (1.038)
  Pallas kernels: 150 us -> 157 us
    pallas_call x1, Pallas kernels: 150 us -> 157 us  [fused_device(): pl.pallas_call(functools.partial(kernel, ep, slots), out_shape=jax.ShapeD...]
where the time goes in v3:
time: 162 us
  Pallas kernels  157 us (97%)
  local copies, waits for them, and re-layouts  5.24 us (3%)
    pallas_call x1, Pallas kernels, fused_device(): pl.pallas_call(functools.partial(kernel, ep, slots), out_shape=jax.ShapeD...  157 us
    unnamed x3, local copies, waits for them, and re-layouts  5.24 us

profile of v3, /device:TPU:0, one launch (start us, length us, event | category | flops | bytes accessed | tf_op | source)
XLA Modules:
  0.0 161.9 jit_solution(16812177370777232937)
XLA Ops:
  0.0 1.5 copy.8.ids
  1.5 1.5 copy.9.rw
  2.9 156.7 %shard_map.73 = bf16[256,2048]{1,0:T(8,128)(2,1)} custom-call(bf16[256,2048]{1,0:T(8,128)(2,1)} %tok.1, f32[1,2048]{1,0:T(1,128)} %bitcast.1, s32[256,2]{1,0:T(8,128)} %copy.8.ids, f32[256,2]{1,0:T(8,128)} %copy.9.rw, bf16[1,2048,512]{2,1,0:T(8,128)(2,1)} %wg.1, bf16[1,2048,512]{2,1,0:T(8,128)(2,1)} %wu.1, bf16[1,512,2048]{2,1,0:T(8,128)(2,1)} %wd.1), custom_call_target="tpu_custom_call" | custom-call | tf_op jit(solution)/shard_map/pallas_call | solution.py:296
  159.6 2.3 %copy.11 = bf16[256,2048]{1,0:T(8,128)(2,1)} copy(bf16[256,2048]{1,0:T(8,128)(2,1)} %shard_map.73) | data formatting | bytes 2097152
